TPU v7x, 128 devices: a whole 4x4x4 slice. The times are simulated.
128 devices in a mesh: rep: 2 (over z_hi), fs: 32 (over z_lo, y, x), tp: 2 (over core).
Axes of the slice: x: 4, y: 4, z: 4 (z_hi: 2, z_lo: 2; z = z_hi * 2 + z_lo), core: 2. Of those that a mesh axis runs over, the one named last changes fastest.
Arguments:
- tokens: bfloat16 [64, 1024, 2048], P(('rep', 'fs'), 'tp'), may hold values from -6 to 6
- mix_gain: float32 [2048], replicated, may hold values from 0.1 to 1.9
- out_gate_w: float32 [2048, 1024], P('fs', 'tp'), may hold values from -0.125 to 0.125
- in_gate_w: float32 [2048, 1024], P('fs', 'tp'), may hold values from -0.125 to 0.125
- value_w: float32 [2048, 1024], P('fs', 'tp'), may hold values from -0.125 to 0.125
- out_gate_scale: float32 [1024], P(('tp', 'fs')), may hold values from 0.28 to 3.5
- in_gate_scale: float32 [1024], P(('tp', 'fs')), may hold values from 0.5 to 2
- value_scale: float32 [1024], P(('tp', 'fs')), may hold values from 0.5 to 2
- mix_taps: float32 [3, 1024], P(None, 'tp'), may hold values from -3.5 to 3.5
- conv_gain: float32 [1024], P('tp'), may hold values from 0.1 to 1.9
- out_proj_w: float32 [1024, 2048], P('tp', 'fs'), may hold values from -0.1875 to 0.1875
- proj_scale: float32 [2048], P('fs'), may hold values from 0.5 to 2
- ffn_gain: float32 [2048], replicated, may hold values from 0.1 to 1.9
- gate_w: float32 [2048, 2816], P('fs', 'tp'), may hold values from -0.125 to 0.125
- up_w: float32 [2048, 2816], P('fs', 'tp'), may hold values from -0.125 to 0.125
- gate_scale: float32 [2816], P(('tp', 'fs')), may hold values from 0.5 to 2
- up_scale: float32 [2816], P(('tp', 'fs')), may hold values from 0.5 to 2
- gate_taps: float32 [3, 2816], P(None, 'tp'), may hold values from -3.5 to 3.5
- up_taps: float32 [3, 2816], P(None, 'tp'), may hold values from -3.5 to 3.5
- gate_bias: float32 [2816], P('tp'), may hold values from -3 to 3
- up_bias: float32 [2816], P('tp'), may hold values from -3 to 3
- down_w: float32 [2816, 2048], P('tp', 'fs'), may hold values from -0.109375 to 0.109375
- down_scale: float32 [2048], P('fs'), may hold values from 0.5 to 2
Outputs:
- layer_out: bfloat16 [64, 1024, 2048], P(('rep', 'fs'), 'tp')
All inputs are finite; a program needn't handle non-finite values.
Results may differ from a plain program's by a relative error of at most 0.02.
Values may be sent and summed in bfloat16 or wider, within the bound.
A program may use at most 128 MiB of HBM per device.

v0:
```python
import jax
import jax.numpy as jnp
from jax import lax
from jax.sharding import PartitionSpec as P

epsilon = 1e-06


def joined_along(parts, dim):
    shape = list(parts.shape[1:])
    shape[dim] *= parts.shape[0]
    return jnp.moveaxis(parts, 0, dim).reshape(shape)


def gather_packed(arrays, axis, dims):
    ravelled = jnp.concatenate([a.reshape(-1) for a in arrays])
    lines, at, done = (lax.all_gather(ravelled, axis), 0, [])
    for a, dim in zip(arrays, dims):
        parts = lines[:, at : at + a.size].reshape(-1, *a.shape)
        done.append(joined_along(parts, dim))
        at += a.size
    return tuple(done)


def side_by_side(arrays, axis, dim, along):
    widths = [a.shape[along] for a in arrays]
    both = jnp.concatenate(arrays, axis=along)
    filled = lax.all_gather(both, axis, axis=dim, tiled=True)
    return tuple(jnp.split(filled, [sum(widths[:k]) for k in range(1, len(widths))], axis=along))


def from_everyone(shard, axis):
    size = lax.axis_size(axis)
    return lax.all_to_all(
        jnp.broadcast_to(shard[None], (size, *shard.shape)), axis, 0, 0, tiled=True
    )


def of_everyone(shard, axis):
    return from_everyone(shard, axis).sum(axis=0)


def collect(shard, axis, dim):
    return joined_along(from_everyone(shard, axis), dim)


def split_up(shard, dim, size):
    before, after = (shard.shape[:dim], shard.shape[dim + 1 :])
    return jnp.moveaxis(shard.reshape(*before, size, -1, *after), dim, 0)


def summed_on_arrival(shard, axis, dim):
    size = lax.axis_size(axis)
    parts = lax.all_to_all(split_up(shard, dim, size), axis, 0, 0, tiled=True)
    return jnp.sum(parts.astype(jnp.float32), axis=0)


def norm_rows(values, gain):
    return values * lax.rsqrt(jnp.mean(values * values, axis=-1, keepdims=True) + epsilon) * gain


def causal_taps(values, taps):
    kernel = taps.shape[0]
    length = values.shape[0]
    padded = jnp.pad(values, ((kernel - 1, 0), (0, 0)))
    total = jnp.zeros(values.shape, jnp.float32)
    for offset in range(kernel):
        total = total + taps[offset] * padded[offset : offset + length]
    return total


def column_block(left, scale_all, piece):
    return jnp.dot(left, piece, preferred_element_type=jnp.float32) * scale_all


def local(
    tokens,
    mix_gain,
    out_gate_w,
    in_gate_w,
    value_w,
    out_gate_scale,
    in_gate_scale,
    value_scale,
    mix_taps,
    conv_gain,
    out_proj_w,
    proj_scale,
    ffn_gain,
    gate_w,
    up_w,
    gate_scale,
    up_scale,
    gate_taps,
    up_taps,
    gate_bias,
    up_bias,
    down_w,
    down_scale,
):
    resid = tokens[0].astype(jnp.float32)
    normed_in = norm_rows(resid, mix_gain).astype(jnp.bfloat16)
    all_rows = lax.all_gather(normed_in, "tp", axis=0, tiled=True)
    whole_outgate, whole_ingate, whole_value, whole_gate, whole_up, whole_proj, whole_down = (
        gather_packed(
            (
                out_gate_scale,
                in_gate_scale,
                value_scale,
                gate_scale,
                up_scale,
                proj_scale,
                down_scale,
            ),
            "fs",
            (0, 0, 0, 0, 0, 0, 0),
        )
    )
    outgate_rows, ingate_rows, value_rows = side_by_side(
        (
            out_gate_w.astype(jnp.bfloat16),
            in_gate_w.astype(jnp.bfloat16),
            value_w.astype(jnp.bfloat16),
        ),
        "fs",
        0,
        1,
    )
    out_gate = (
        jnp.dot(all_rows, outgate_rows, preferred_element_type=jnp.float32) * whole_outgate
    ).astype(jnp.bfloat16)
    in_gate = (
        jnp.dot(all_rows, ingate_rows, preferred_element_type=jnp.float32) * whole_ingate
    ).astype(jnp.bfloat16)
    value_in = (
        jnp.dot(all_rows, value_rows, preferred_element_type=jnp.float32) * whole_value
    ).astype(jnp.bfloat16)
    mixed_in = in_gate.astype(jnp.float32) * value_in.astype(jnp.float32)
    conv_out = (out_gate.astype(jnp.float32) * causal_taps(mixed_in, mix_taps)).astype(jnp.bfloat16)
    conv_float = conv_out.astype(jnp.float32)
    channels = conv_float.shape[1] * lax.axis_size("tp")
    sumsq = of_everyone(jnp.sum(conv_float * conv_float, axis=1), "tp")
    mixed = (conv_float * lax.rsqrt(sumsq / channels + epsilon)[:, None] * conv_gain).astype(
        jnp.bfloat16
    )
    partial_mix = (lambda piece, start: column_block(mixed, whole_proj, piece))(
        collect(out_proj_w.astype(jnp.bfloat16), "fs", 1), jnp.int32(0)
    )
    summed = summed_on_arrival(partial_mix.astype(jnp.bfloat16), "tp", 0)
    first = (resid + summed).astype(jnp.bfloat16)
    resid_two = first.astype(jnp.float32)
    normed_ffn = norm_rows(resid_two, ffn_gain).astype(jnp.bfloat16)
    ffn_all = lax.all_gather(normed_ffn, "tp", axis=0, tiled=True)
    gate_cast = gate_w.astype(jnp.bfloat16)
    up_cast = up_w.astype(jnp.bfloat16)
    pieces = side_by_side((gate_cast, up_cast), "fs", 0, 1)
    gate_sum = jnp.dot(ffn_all, pieces[0], preferred_element_type=jnp.float32)
    up_sum = jnp.dot(ffn_all, pieces[1], preferred_element_type=jnp.float32)
    gate_pre = (gate_sum * whole_gate).astype(jnp.bfloat16)
    up_pre = (up_sum * whole_up).astype(jnp.bfloat16)
    gate_act = causal_taps(gate_pre.astype(jnp.float32), gate_taps) + gate_bias
    up_act = causal_taps(up_pre.astype(jnp.float32), up_taps) + up_bias
    hidden = (jax.nn.silu(gate_act) * up_act).astype(jnp.bfloat16)
    partial_down = column_block(
        hidden, whole_down, lax.all_gather(down_w.astype(jnp.bfloat16), "fs", axis=1, tiled=True)
    )
    summed_two = summed_on_arrival(partial_down.astype(jnp.bfloat16), "tp", 0)
    return (resid_two + summed_two).astype(jnp.bfloat16)[None]


def solution(mesh):
    placed = (
        P(("rep", "fs"), "tp", None),
        P(),
        P("fs", "tp"),
        P("fs", "tp"),
        P("fs", "tp"),
        P(("tp", "fs")),
        P(("tp", "fs")),
        P(("tp", "fs")),
        P(None, "tp"),
        P("tp"),
        P("tp", "fs"),
        P("fs"),
        P(),
        P("fs", "tp"),
        P("fs", "tp"),
        P(("tp", "fs")),
        P(("tp", "fs")),
        P(None, "tp"),
        P(None, "tp"),
        P("tp"),
        P("tp"),
        P("tp", "fs"),
        P("fs"),
    )
    return jax.shard_map(
        local, mesh=mesh, in_specs=placed, out_specs=P(("rep", "fs"), "tp", None), check_vma=False
    )
```

profile of v0, /device:TPU:1, one launch (start us, length us, event | category | flops | bytes accessed | tf_op | source)
XLA Modules:
  0.0 658.0 jit_solution(3495908413047542810)
XLA Ops:
  6.5 2.1 fusion.11
  8.8 3.5 fusion.13
  12.4 0.0 all-gather.9.cloned.1.call-start
  12.5 0.7 pad_maximum_fusion.1
  13.2 0.7 dynamic-slice
  14.6 0.1 concatenate.10
  14.7 0.3 dynamic-update-slice
  15.0 135.7 %all-reduce.3 = f32[8448]{0:T(1024)S(1)} all-reduce(f32[8448]{0:T(1024)S(1)} %dynamic-update-slice), channel_id=2, replica_groups=mesh['rep'=2,'fs'=32,'tp'=2] {'fs'}, use_global_device_ids=true, to_apply=%add.3 | all-reduce | flops 8448 | bytes 67584
  150.7 0.1 reshape.57
  150.8 0.1 fusion.57
  150.9 0.1 mul.243
  150.9 0.1 mul.240
  151.0 0.1 mul.235
  151.2 25.6 %all-gather.9.cloned.1.call-done = bf16[2048,1536]{1,0:T(8,128)(2,1)} async-done(((bf16[64,1536]{1,0:T(8,128)(2,1)}), bf16[2048,1536]{1,0:T(8,128)(2,1)}) %all-gather.9.cloned.1.call-update) | async-done | bytes 6291472 | tf_op jit(solution)/shard_map/all_gather | solution.py:28
  176.8 5.4 multiply_convert_fusion.6
  182.1 0.5 copy-done.23
  182.6 2.4 convert_multiply_fusion.4
  185.0 3.1 fusion.32
  188.1 24.5 %all_to_all.21 = f32[2,1,1024]{2,1,0:T(1,128)S(1)} all-to-all(f32[2,1,1024]{2,1,0:T(1,128)S(1)} %broadcast_in_dim.4), channel_id=1, replica_groups=mesh['rep'=2,'fs'=32,'tp'=2] {'tp'}, dimensions={0} | all-to-all | bytes 16384 | tf_op jit(solution)/shard_map/all_to_all | solution.py:34
  212.7 1.6 broadcast_in_dim.5
  214.2 6.8 %all-to-all-start.1 = ((bf16[32,512,64]{1,2,0:T(8,128)(2,1)}), bf16[32,512,64]{1,2,0:T(8,128)(2,1)S(1)}, u32[]{:S(2)}, u32[]{:S(2)}) async-start(bf16[32,512,64]{1,2,0:T(8,128)(2,1)} %broadcast_in_dim.5), calls=%async_computation.1 | async-start | bytes 4194304 | tf_op jit(solution)/shard_map/all_to_all | solution.py:34
  221.0 0.1 fusion.58
  221.1 0.1 mul.260
  221.2 26.7 %all-to-all-done.1 = bf16[32,512,64]{1,2,0:T(8,128)(2,1)S(1)} async-done(((bf16[32,512,64]{1,2,0:T(8,128)(2,1)}), bf16[32,512,64]{1,2,0:T(8,128)(2,1)S(1)}, u32[]{:S(2)}, u32[]{:S(2)}) %all-to-all-start.1) | async-done | bytes 2097184 | tf_op jit(solution)/shard_map/all_to_all | solution.py:34
  247.9 2.6 multiply_convert_fusion.1
  250.5 8.9 %all_to_all.22 = bf16[2,512,2048]{2,1,0:T(8,128)(2,1)S(1)} all-to-all(bf16[2,512,2048]{2,1,0:T(8,128)(2,1)S(1)} %bitcast.45), channel_id=1, replica_groups=mesh['rep'=2,'fs'=32,'tp'=2] {'tp'}, dimensions={0} | all-to-all | bytes 8388608 | tf_op jit(solution)/shard_map/all_to_all | solution.py:54
  259.4 1.0 convert_reduce_fusion.1
  260.4 0.6 copy-done.2
  261.0 0.7 fusion.16
  261.7 1.3 copy-done
  263.0 2.0 fusion.18
  265.2 0.8 pad_maximum_fusion
  266.1 0.7 convert_element_type.142
  266.8 0.1 fusion.56
  266.9 0.1 mul.270
  267.0 0.1 mul.283
  267.1 0.1 mul.294
  267.2 0.1 slice_reduce_fusion.2
  267.2 13.0 %all-gather.11.cloned.1.call-done = bf16[1024,2048]{1,0:T(8,128)(2,1)} async-done(((bf16[512,2048]{1,0:T(8,128)(2,1)}), bf16[1024,2048]{1,0:T(8,128)(2,1)}) %all-gather.11.cloned.1.call-update) | async-done | bytes 4194320 | tf_op jit(solution)/shard_map/all_gather | solution.py:153
  280.3 155.1 %all-gather.13.cloned.1.call-done = bf16[2048,2816]{1,0:T(8,128)(2,1)} async-done(((bf16[64,2816]{1,0:T(8,128)(2,1)}), bf16[2048,2816]{1,0:T(8,128)(2,1)}) %all-gather.13.cloned.1.call-update) | async-done | bytes 11534352 | tf_op jit(solution)/shard_map/all_gather | solution.py:28
  435.4 11.8 %fusion.20 = f32[1024,1408]{1,0:T(8,128)} fusion(bf16[1024,2048]{1,0:T(8,128)(2,1)} %all-gather.11.cloned.1.call-done, bf16[2048,2816]{1,0:T(8,128)(2,1)} %all-gather.13.cloned.1.call-done, f32[1408]{0:T(1024)S(1)} %mul.270), kind=kOutput, calls=%fused_computation.28 | convolution fusion | flops 5909905408 | bytes 15734272 | tf_op jit(solution)/shard_map/dot_general | solution.py:157
  447.2 8.5 %fusion.23 = f32[1024,1408]{1,0:T(8,128)} fusion(bf16[1024,2048]{1,0:T(8,128)(2,1)S(1)} %copy-done.24, bf16[2048,2816]{1,0:T(8,128)(2,1)S(1)} %copy-done.21, f32[1408]{0:T(1024)S(1)} %mul.283), kind=kOutput, calls=%fused_computation.29 | convolution fusion | flops 5909905408 | bytes 15736832 | tf_op jit(solution)/shard_map/dot_general | solution.py:158
  455.7 139.5 %all-gather.15.cloned.1.call-done = bf16[1408,2048]{0,1:T(8,128)(2,1)} async-done(((bf16[1408,64]{0,1:T(8,128)(2,1)}), bf16[1408,2048]{0,1:T(8,128)(2,1)}) %all-gather.15.cloned.1.call-update) | async-done | bytes 5767184 | tf_op jit(solution)/shard_map/all_gather | solution.py:165
  595.2 23.3 %multiply_convert_fusion = bf16[1024,2048]{1,0:T(8,128)(2,1)} fusion(bf16[1408,2048]{0,1:T(8,128)(2,1)} %all-gather.15.cloned.1.call-done, f32[2048]{0:T(1024)S(1)} %mul.294, f32[1024,1408]{1,0:T(8,128)} %fusion.23, f32[1024,1408]{1,0:T(8,128)} %fusion.20, f32[1408]{0:T(1024)S(1)} %copy-done.25, f32[1408]{0:T(1024)S(1)} %get-tuple-element.9, ...), kind=kOutput, calls=%fused_computation.1 | convolution fusion | flops 5935726592 | bytes 21549056 | tf_op jit(solution)/shard_map/dot_general | solution.py:73
  618.5 28.2 %all_to_all.23 = bf16[2,512,2048]{2,1,0:T(8,128)(2,1)S(1)} all-to-all(bf16[2,512,2048]{2,1,0:T(8,128)(2,1)} %bitcast.44), channel_id=1, replica_groups=mesh['rep'=2,'fs'=32,'tp'=2] {'tp'}, dimensions={0} | all-to-all | bytes 8388608 | tf_op jit(solution)/shard_map/all_to_all | solution.py:54
  646.7 1.0 convert_reduce_fusion
  647.7 1.2 copy-done.1
  648.9 2.5 fusion.19
  (77 shorter events, 0.5 us)
Async XLA Ops:
  6.5 5.9 copy-start.6
  6.5 5.9 copy-start.7
  6.5 5.9 copy-start.8
  6.5 144.6 %all-gather.7.cloned.1.call-start = ((), (), s32[]{:S(2)}) async-start(), calls=%async_computation.4 | async-start | bytes 6291456 | tf_op jit(solution)/shard_map/all_gather | solution.py:103
  8.7 4.5 copy-start.28
  8.7 5.9 copy-start.14
  8.7 5.9 copy-start.15
  8.7 5.9 copy-start.16
  8.7 5.9 copy-start.17
  8.7 5.9 copy-start.18
  8.7 5.9 copy-start.19
  8.7 5.9 copy-start.20
  8.8 142.3 %copy-start.9 = (f32[512,64]{0,1:T(8,128)S(1)}, f32[512,64]{0,1:T(8,128)}, u32[]{:S(2)}) copy-start(f32[512,64]{0,1:T(8,128)} %param.33) | copy-start | bytes 393220
  8.8 142.4 %copy-start.13 = (f32[3,512]{1,0:T(4,128)S(1)}, f32[3,512]{1,0:T(4,128)}, u32[]{:S(2)}) copy-start(f32[3,512]{1,0:T(4,128)} %param.31) | copy-start | bytes 18436
  12.4 164.4 %all-gather.9.cloned.1.call-start = ((), (), s32[]{:S(2)}) async-start(), calls=%async_computation.5 | async-start | bytes 6488064 | tf_op jit(solution)/shard_map/all_gather | solution.py:28
  176.8 5.4 copy-start.22
  176.8 5.9 copy-start.23
  188.1 59.8 %copy-start.27 = (f32[512]{0:T(512)S(1)}, f32[512]{0:T(512)}, u32[]{:S(2)}) copy-start(f32[512]{0:T(512)} %param.32) | copy-start | bytes 6148
  214.2 33.7 %all-to-all-start.1 = ((bf16[32,512,64]{1,2,0:T(8,128)(2,1)}), bf16[32,512,64]{1,2,0:T(8,128)(2,1)S(1)}, u32[]{:S(2)}, u32[]{:S(2)}) async-start(bf16[32,512,64]{1,2,0:T(8,128)(2,1)} %broadcast_in_dim.5), calls=%async_computation.1 | async-start | bytes 4194304 | tf_op jit(solution)/shard_map/all_to_all | solution.py:34
  221.0 59.3 %all-gather.11.cloned.1.call-start = ((), (), s32[]{:S(2)}) async-start(), calls=%async_computation.6 | async-start | bytes 6291456 | tf_op jit(solution)/shard_map/all_gather | solution.py:153
  259.4 1.6 copy-start.2
  261.0 2.0 copy-start
  261.0 2.0 copy-start.12
  263.0 2.1 copy-start.3
  263.0 2.2 copy-start.4
  265.1 1.0 copy-start.5
  265.1 2.1 copy-start.10
  265.1 2.1 copy-start.11
  265.1 170.3 %all-gather.13.cloned.1.call-start = ((), (), s32[]{:S(2)}) async-start(), calls=%async_computation.7 | async-start | bytes 11894784 | tf_op jit(solution)/shard_map/all_gather | solution.py:28
  266.0 329.2 %all-gather.15.cloned.1.call-start = ((), (), s32[]{:S(2)}) async-start(), calls=%async_computation.8 | async-start | bytes 5947392 | tf_op jit(solution)/shard_map/all_gather | solution.py:165
  435.4 11.8 %copy-start.21 = (bf16[2048,2816]{1,0:T(8,128)(2,1)S(1)}, bf16[2048,2816]{1,0:T(8,128)(2,1)}, u32[]{:S(2)}) copy-start(bf16[2048,2816]{1,0:T(8,128)(2,1)} %all-gather.13.cloned.1.call-done) | copy-start | bytes 34603012
  435.4 11.8 %copy-start.24 = (bf16[1024,2048]{1,0:T(8,128)(2,1)S(1)}, bf16[1024,2048]{1,0:T(8,128)(2,1)}, u32[]{:S(2)}) copy-start(bf16[1024,2048]{1,0:T(8,128)(2,1)} %all-gather.11.cloned.1.call-done) | copy-start | bytes 12582916
  447.2 148.0 %copy-start.25 = (f32[1408]{0:T(1024)S(1)}, f32[1408]{0:T(1024)}, u32[]{:S(2)}) copy-start(f32[1408]{0:T(1024)} %param.43) | copy-start | bytes 16900
  447.2 148.0 %copy-start.26 = (f32[1408]{0:T(1024)S(1)}, f32[1408]{0:T(1024)}, u32[]{:S(2)}) copy-start(f32[1408]{0:T(1024)} %param.42) | copy-start | bytes 16900
  646.7 2.2 copy-start.1
Sparse Core Ops, SparseCore 0:
  12.5 19.9 all-gather.6
  34.1 142.5 all-gather.8
  265.2 15.0 all-gather.10
  281.8 153.5 all-gather.12
  436.9 158.2 all-gather.14
where the time goes:
time: 658 us
  waiting for transfers between devices  360 us (55%)
  blocking collectives  197 us (30%)
  matrix products  57 us (9%)
  other arithmetic  15.1 us (2%)
  between operations  14.3 us (2%)
  local copies, waits for them, and re-layouts  7.36 us (1%)
  starting transfers between devices  6.92 us (1%)
    all_gather x2, waiting for transfers between devices, side_by_side(): filled = lax.all_gather(both, axis, axis=dim, tiled=True)  181 us
    all_gather x1, waiting for transfers between devices, local(): lax.all_gather(down_w.astype(jnp.bfloat16), 'fs', axis=1, tiled=True)  139 us
    unnamed x1, blocking collectives  136 us
    all_to_all x2, blocking collectives, summed_on_arrival(): parts = lax.all_to_all(split_up(shard, dim, size), axis, 0, 0, tiled=True)  37.1 us
    all_to_all x1, waiting for transfers between devices, from_everyone(): lax.all_to_all(jnp.broadcast_to(shard[None], (size, *shard.shape)), axis,...  26.7 us
    dot_general x2, matrix products, column_block(): return jnp.dot(left, piece, preferred_element_type=jnp.float32) * scale_all  25.9 us
    all_to_all x1, blocking collectives, from_everyone(): lax.all_to_all(jnp.broadcast_to(shard[None], (size, *shard.shape)), axis,...  24.5 us
  transfers between devices with their start and end apart: 6, of which 5 were waited for; matrix products, arithmetic and copies ran while one was open for 4% of the time, Pallas kernels for 0%

commit v1 on v0

--- a/solution.py
+++ b/solution.py
@@ -162,7 +162,14 @@
     up_act = causal_taps(up_pre.astype(jnp.float32), up_taps) + up_bias
     hidden = (jax.nn.silu(gate_act) * up_act).astype(jnp.bfloat16)
     partial_down = column_block(
-        hidden, whole_down, lax.all_gather(down_w.astype(jnp.bfloat16), "fs", axis=1, tiled=True)
+        hidden,
+        whole_down,
+        jnp.concatenate(
+            lax.all_to_all(
+                jnp.stack([down_w.astype(jnp.bfloat16)] * lax.axis_size("fs")), "fs", 0, 0
+            ),
+            axis=1,
+        ),
     )
     summed_two = summed_on_arrival(partial_down.astype(jnp.bfloat16), "tp", 0)
     return (resid_two + summed_two).astype(jnp.bfloat16)[None]

time: 658 us -> 567 us (0.86)
  waiting for transfers between devices: 360 us -> 264 us
    all_gather x1 -> x0, waiting for transfers between devices: 139 us -> none  [local(): lax.all_gather(down_w.astype(jnp.bfloat16), 'fs', axis=1, tiled=True)]
    all_gather x2, waiting for transfers between devices: 181 us -> 232 us  [side_by_side(): filled = lax.all_gather(both, axis, axis=dim, tiled=True)]
    all_gather x1, waiting for transfers between devices: 13 us -> 5.21 us  [local(): ffn_all = lax.all_gather(normed_ffn, 'tp', axis=0, tiled=True)]
  transfers between devices with their start and end apart: 6 -> 6, of which waited for: 5 -> 4; matrix products, arithmetic and copies ran while one was open for 4% -> 5% of each run, Pallas kernels for 0% -> 0%
where the time goes in v1:
time: 567 us; the launch traced here: 566 us
  waiting for transfers between devices  264 us (47%)
  blocking collectives  194 us (34%)
  matrix products  56.7 us (10%)
  other arithmetic  14.4 us (3%)
  between operations  14.2 us (3%)
  starting transfers between devices  12.4 us (2%)
  local copies, waits for them, and re-layouts  10.5 us (2%)
    all_gather x2, waiting for transfers between devices, side_by_side(): filled = lax.all_gather(both, axis, axis=dim, tiled=True)  232 us
    unnamed x1, blocking collectives  136 us
    all_to_all x2, blocking collectives, summed_on_arrival(): parts = lax.all_to_all(split_up(shard, dim, size), axis, 0, 0, tiled=True)  33.3 us
    all_to_all x1, waiting for transfers between devices, from_everyone(): lax.all_to_all(jnp.broadcast_to(shard[None], (size, *shard.shape)), axis,...  26.7 us
    dot_general x2, matrix products, column_block(): return jnp.dot(left, piece, preferred_element_type=jnp.float32) * scale_all  25.6 us
    all_to_all x1, blocking collectives, from_everyone(): lax.all_to_all(jnp.broadcast_to(shard[None], (size, *shard.shape)), axis,...  24.4 us
    dot_general x1, matrix products, local(): gate_sum = jnp.dot(ffn_all, pieces[0], preferred_element_type=jnp.float32)  11.8 us
  transfers between devices with their start and end apart: 6, of which 4 were waited for; matrix products, arithmetic and copies ran while one was open for 5% of the time, Pallas kernels for 0%

profile of v1, /device:TPU:1, one launch (start us, length us, event | category | flops | bytes accessed | tf_op | source)
XLA Modules:
  0.0 565.9 jit_solution(13670145936547688348)
XLA Ops:
  6.5 2.1 fusion.11
  8.8 3.5 fusion.13
  12.4 0.0 all-gather.8.cloned.1.call-start
  12.5 0.7 pad_maximum_fusion.1
  13.2 0.6 dynamic-slice
  14.5 0.1 concatenate.10
  14.6 0.3 dynamic-update-slice
  14.9 136.1 %all-reduce.3 = f32[8448]{0:T(1024)S(1)} all-reduce(f32[8448]{0:T(1024)S(1)} %dynamic-update-slice), channel_id=2, replica_groups=mesh['rep'=2,'fs'=32,'tp'=2] {'fs'}, use_global_device_ids=true, to_apply=%add.3 | all-reduce | flops 8448 | bytes 67584
  151.0 0.1 reshape.67
  151.1 0.1 fusion.57
  151.2 0.1 mul.243
  151.2 0.1 mul.240
  151.3 0.1 mul.235
  151.5 25.2 %all-gather.8.cloned.1.call-done = bf16[2048,1536]{1,0:T(8,128)(2,1)} async-done(((bf16[64,1536]{1,0:T(8,128)(2,1)}), bf16[2048,1536]{1,0:T(8,128)(2,1)}) %all-gather.8.cloned.1.call-update) | async-done | bytes 6291472 | tf_op jit(solution)/shard_map/all_gather | solution.py:28
  176.7 5.4 multiply_convert_fusion.6
  182.0 0.5 copy-done.23
  182.5 2.4 convert_multiply_fusion.4
  184.9 3.1 fusion.32
  188.0 24.4 %all_to_all.26 = f32[2,1,1024]{2,1,0:T(1,128)S(1)} all-to-all(f32[2,1,1024]{2,1,0:T(1,128)S(1)} %broadcast_in_dim.4), channel_id=1, replica_groups=mesh['rep'=2,'fs'=32,'tp'=2] {'tp'}, dimensions={0} | all-to-all | bytes 16384 | tf_op jit(solution)/shard_map/all_to_all | solution.py:34
  212.4 1.6 broadcast_in_dim.5
  213.9 7.2 %all-to-all-start.1 = ((bf16[32,512,64]{1,2,0:T(8,128)(2,1)}), bf16[32,512,64]{1,2,0:T(8,128)(2,1)S(1)}, u32[]{:S(2)}, u32[]{:S(2)}) async-start(bf16[32,512,64]{1,2,0:T(8,128)(2,1)} %broadcast_in_dim.5), calls=%async_computation.1 | async-start | bytes 4194304 | tf_op jit(solution)/shard_map/all_to_all | solution.py:34
  221.2 0.1 fusion.58
  221.2 0.1 mul.260
  221.4 26.7 %all-to-all-done.1 = bf16[32,512,64]{1,2,0:T(8,128)(2,1)S(1)} async-done(((bf16[32,512,64]{1,2,0:T(8,128)(2,1)}), bf16[32,512,64]{1,2,0:T(8,128)(2,1)S(1)}, u32[]{:S(2)}, u32[]{:S(2)}) %all-to-all-start.1) | async-done | bytes 2097184 | tf_op jit(solution)/shard_map/all_to_all | solution.py:34
  248.1 2.6 multiply_convert_fusion.1
  250.7 8.9 %all_to_all.27 = bf16[2,512,2048]{2,1,0:T(8,128)(2,1)S(1)} all-to-all(bf16[2,512,2048]{2,1,0:T(8,128)(2,1)S(1)} %bitcast.48), channel_id=1, replica_groups=mesh['rep'=2,'fs'=32,'tp'=2] {'tp'}, dimensions={0} | all-to-all | bytes 8388608 | tf_op jit(solution)/shard_map/all_to_all | solution.py:54
  259.6 1.0 convert_reduce_fusion.1
  260.6 0.6 copy-done.2
  261.2 0.7 fusion.16
  261.9 1.3 copy-done
  263.1 2.0 fusion.18
  265.3 0.8 pad_maximum_fusion
  266.2 3.2 stack.2
  269.4 5.0 all-to-all-start.3
  274.4 0.1 fusion.56
  274.5 0.1 mul.270
  274.6 0.1 mul.283
  274.7 0.1 mul.294
  274.8 0.1 slice_reduce_fusion.2
  274.9 5.2 all-gather.10.cloned.1.call-done
  280.1 206.9 %all-gather.12.cloned.1.call-done = bf16[2048,2816]{1,0:T(8,128)(2,1)} async-done(((bf16[64,2816]{1,0:T(8,128)(2,1)}), bf16[2048,2816]{1,0:T(8,128)(2,1)}) %all-gather.12.cloned.1.call-update) | async-done | bytes 11534352 | tf_op jit(solution)/shard_map/all_gather | solution.py:28
  487.0 11.8 %fusion.20 = f32[1024,1408]{1,0:T(8,128)} fusion(bf16[1024,2048]{1,0:T(8,128)(2,1)} %all-gather.10.cloned.1.call-done, bf16[2048,2816]{1,0:T(8,128)(2,1)} %all-gather.12.cloned.1.call-done, f32[1408]{0:T(1024)S(1)} %mul.270), kind=kOutput, calls=%fused_computation.28 | convolution fusion | flops 5909905408 | bytes 15734272 | tf_op jit(solution)/shard_map/dot_general | solution.py:157
  498.8 8.5 %fusion.23 = f32[1024,1408]{1,0:T(8,128)} fusion(bf16[1024,2048]{1,0:T(8,128)(2,1)S(1)} %copy-done.24, bf16[2048,2816]{1,0:T(8,128)(2,1)S(1)} %copy-done.21, f32[1408]{0:T(1024)S(1)} %mul.283), kind=kOutput, calls=%fused_computation.29 | convolution fusion | flops 5909905408 | bytes 15736832 | tf_op jit(solution)/shard_map/dot_general | solution.py:158
  507.3 23.0 %multiply_convert_fusion = bf16[1024,2048]{1,0:T(8,128)(2,1)} fusion(bf16[1408,2048]{0,1:T(8,128)(2,1)} %bitcast.10, f32[2048]{0:T(1024)S(1)} %mul.294, f32[1024,1408]{1,0:T(8,128)} %fusion.23, f32[1024,1408]{1,0:T(8,128)} %fusion.20, f32[1408]{0:T(1024)S(1)} %copy-done.25, f32[1408]{0:T(1024)S(1)} %get-tuple-element.9, f32[1408]{0:T(1024)S(1)} %get-tuple-element.10, ...), kind=kOutput, calls=%fused_computation.1 | convolution fusion | flops 5935726592 | bytes 21549056 | tf_op jit(solution)/shard_map/dot_general | solution.py:73
  530.3 24.4 %all_to_all.28 = bf16[2,512,2048]{2,1,0:T(8,128)(2,1)S(1)} all-to-all(bf16[2,512,2048]{2,1,0:T(8,128)(2,1)} %bitcast.47), channel_id=1, replica_groups=mesh['rep'=2,'fs'=32,'tp'=2] {'tp'}, dimensions={0} | all-to-all | bytes 8388608 | tf_op jit(solution)/shard_map/all_to_all | solution.py:54
  554.7 1.0 convert_reduce_fusion
  555.6 1.2 copy-done.1
  556.8 2.5 fusion.19
  (77 shorter events, 0.5 us)
Async XLA Ops:
  6.5 5.9 %copy-start.6 = (f32[64,512]{1,0:T(8,128)S(1)}, f32[64,512]{1,0:T(8,128)}, u32[]{:S(2)}) copy-start(f32[64,512]{1,0:T(8,128)} %param.25) | copy-start | bytes 393220
  6.5 5.9 %copy-start.7 = (f32[64,512]{1,0:T(8,128)S(1)}, f32[64,512]{1,0:T(8,128)}, u32[]{:S(2)}) copy-start(f32[64,512]{1,0:T(8,128)} %param.26) | copy-start | bytes 393220
  6.5 5.9 %copy-start.8 = (f32[64,512]{1,0:T(8,128)S(1)}, f32[64,512]{1,0:T(8,128)}, u32[]{:S(2)}) copy-start(f32[64,512]{1,0:T(8,128)} %param.27) | copy-start | bytes 393220
  6.5 144.9 %all-gather.6.cloned.1.call-start = ((), (), s32[]{:S(2)}) async-start(), calls=%async_computation.5 | async-start | bytes 6291456 | tf_op jit(solution)/shard_map/all_gather | solution.py:103
  8.7 4.5 copy-start.28
  8.7 5.8 %copy-start.14 = (f32[16]{0:T(128)S(1)}, f32[16]{0:T(128)}, u32[]{:S(2)}) copy-start(f32[16]{0:T(128)} %param.28) | copy-start | bytes 196
  8.7 5.8 %copy-start.15 = (f32[16]{0:T(128)S(1)}, f32[16]{0:T(128)}, u32[]{:S(2)}) copy-start(f32[16]{0:T(128)} %param.29) | copy-start | bytes 196
  8.7 5.8 %copy-start.16 = (f32[16]{0:T(128)S(1)}, f32[16]{0:T(128)}, u32[]{:S(2)}) copy-start(f32[16]{0:T(128)} %param.30) | copy-start | bytes 196
  8.7 5.8 %copy-start.17 = (f32[44]{0:T(128)S(1)}, f32[44]{0:T(128)}, u32[]{:S(2)}) copy-start(f32[44]{0:T(128)} %param.38) | copy-start | bytes 532
  8.7 5.8 %copy-start.18 = (f32[44]{0:T(128)S(1)}, f32[44]{0:T(128)}, u32[]{:S(2)}) copy-start(f32[44]{0:T(128)} %param.39) | copy-start | bytes 532
  8.7 5.8 %copy-start.19 = (f32[64]{0:T(128)S(1)}, f32[64]{0:T(128)}, u32[]{:S(2)}) copy-start(f32[64]{0:T(128)} %param.34) | copy-start | bytes 772
  8.7 5.8 %copy-start.20 = (f32[64]{0:T(128)S(1)}, f32[64]{0:T(128)}, u32[]{:S(2)}) copy-start(f32[64]{0:T(128)} %param.45) | copy-start | bytes 772
  8.8 142.6 %copy-start.9 = (f32[512,64]{0,1:T(8,128)S(1)}, f32[512,64]{0,1:T(8,128)}, u32[]{:S(2)}) copy-start(f32[512,64]{0,1:T(8,128)} %param.33) | copy-start | bytes 393220
  8.8 142.7 %copy-start.13 = (f32[3,512]{1,0:T(4,128)S(1)}, f32[3,512]{1,0:T(4,128)}, u32[]{:S(2)}) copy-start(f32[3,512]{1,0:T(4,128)} %param.31) | copy-start | bytes 18436
  12.4 164.3 %all-gather.8.cloned.1.call-start = ((), (), s32[]{:S(2)}) async-start(), calls=%async_computation.6 | async-start | bytes 6488064 | tf_op jit(solution)/shard_map/all_gather | solution.py:28
  176.6 5.4 copy-start.22
  176.6 5.9 %copy-start.23 = (bf16[1024,2048]{1,0:T(8,128)(2,1)S(1)}, bf16[1024,2048]{1,0:T(8,128)(2,1)}, u32[]{:S(2)}) copy-start(bf16[1024,2048]{1,0:T(8,128)(2,1)} %all-gather.6.cloned.1.call-done) | copy-start | bytes 12582916
  188.0 60.1 %copy-start.27 = (f32[512]{0:T(512)S(1)}, f32[512]{0:T(512)}, u32[]{:S(2)}) copy-start(f32[512]{0:T(512)} %param.32) | copy-start | bytes 6148
  213.9 34.1 %all-to-all-start.1 = ((bf16[32,512,64]{1,2,0:T(8,128)(2,1)}), bf16[32,512,64]{1,2,0:T(8,128)(2,1)S(1)}, u32[]{:S(2)}, u32[]{:S(2)}) async-start(bf16[32,512,64]{1,2,0:T(8,128)(2,1)} %broadcast_in_dim.5), calls=%async_computation.1 | async-start | bytes 4194304 | tf_op jit(solution)/shard_map/all_to_all | solution.py:34
  221.1 59.0 %all-gather.10.cloned.1.call-start = ((), (), s32[]{:S(2)}) async-start(), calls=%async_computation.7 | async-start | bytes 6291456 | tf_op jit(solution)/shard_map/all_gather | solution.py:153
  259.6 1.6 copy-start.2
  261.2 2.0 copy-start
  261.2 2.0 copy-start.12
  263.1 2.1 copy-start.3
  263.1 2.1 copy-start.4
  265.2 1.0 copy-start.5
  265.2 221.8 %all-gather.12.cloned.1.call-start = ((), (), s32[]{:S(2)}) async-start(), calls=%async_computation.8 | async-start | bytes 11894784 | tf_op jit(solution)/shard_map/all_gather | solution.py:28
  269.4 5.4 copy-start.10
  269.4 5.4 copy-start.11
  269.4 237.9 %all-to-all-start.3 = ((bf16[32,1408,64]{1,2,0:T(8,128)(2,1)}), bf16[32,1408,64]{1,2,0:T(8,128)(2,1)}, u32[]{:S(2)}, u32[]{:S(2)}) async-start(bf16[32,1408,64]{1,2,0:T(8,128)(2,1)} %stack.2), calls=%async_computation.3 | async-start | bytes 11534336 | tf_op jit(solution)/shard_map/all_to_all | solution.py:168
  487.0 11.8 %copy-start.21 = (bf16[2048,2816]{1,0:T(8,128)(2,1)S(1)}, bf16[2048,2816]{1,0:T(8,128)(2,1)}, u32[]{:S(2)}) copy-start(bf16[2048,2816]{1,0:T(8,128)(2,1)} %all-gather.12.cloned.1.call-done) | copy-start | bytes 34603012
  487.0 11.8 %copy-start.24 = (bf16[1024,2048]{1,0:T(8,128)(2,1)S(1)}, bf16[1024,2048]{1,0:T(8,128)(2,1)}, u32[]{:S(2)}) copy-start(bf16[1024,2048]{1,0:T(8,128)(2,1)} %all-gather.10.cloned.1.call-done) | copy-start | bytes 12582916
  498.8 8.5 %copy-start.25 = (f32[1408]{0:T(1024)S(1)}, f32[1408]{0:T(1024)}, u32[]{:S(2)}) copy-start(f32[1408]{0:T(1024)} %param.43) | copy-start | bytes 16900
  498.8 8.5 %copy-start.26 = (f32[1408]{0:T(1024)S(1)}, f32[1408]{0:T(1024)}, u32[]{:S(2)}) copy-start(f32[1408]{0:T(1024)} %param.42) | copy-start | bytes 16900
  554.6 2.2 copy-start.1
Sparse Core Ops, SparseCore 0:
  12.5 19.9 all-gather.5
  34.1 142.4 all-gather.7
  265.3 14.7 all-gather.9
  281.6 205.3 all-gather.11
